TPU v7x, 512 devices: a whole 4x4x16 slice. The times are simulated.
512 devices in a mesh: rep: 2 (over z_hi), fs: 32 (over z_lo, y), tp: 8 (over x, core).
Axes of the slice: x: 4, y: 4, z: 16 (z_hi: 2, z_lo: 8; z = z_hi * 8 + z_lo), core: 2. Of those that a mesh axis runs over, the one named last changes fastest.
Arguments:
- tokens_in: bfloat16 [16384, 2048], P(('rep', 'fs', 'tp')), may hold values from -6 to 6
- norm_gains: float32 [3, 2048], replicated, may hold values from 0.1 to 1.9
- gate_w: float32 [2048, 3072], P('fs', 'tp'), may hold values from -0.125 to 0.125
- gate_scale: float32 [3072], P('tp'), may hold values from 0.5 to 2
- up_w: float32 [2048, 3072], P('fs', 'tp'), may hold values from -0.125 to 0.125
- up_scale: float32 [3072], P('tp'), may hold values from 0.5 to 2
- down_w: float32 [3072, 2048], P('tp', 'fs'), may hold values from -0.109375 to 0.109375
- down_scale: float32 [2048], P('fs'), may hold values from 0.5 to 2
- query_w: float32 [2048, 2048], P('fs', 'tp'), may hold values from -0.125 to 0.125
- query_scale: float32 [2048], P('tp'), may hold values from 0.5 to 2
- key_w: float32 [2048, 2048], P('fs', 'tp'), may hold values from -0.125 to 0.125
- key_scale: float32 [2048], P('tp'), may hold values from 0.5 to 2
- value_w: float32 [2048, 2048], P('fs', 'tp'), may hold values from -0.125 to 0.125
- value_scale: float32 [2048], P('tp'), may hold values from 0.5 to 2
- out_w: float32 [2048, 2048], P('tp', 'fs'), may hold values from -0.125 to 0.125
- out_scale: float32 [2048], P('fs'), may hold values from 0.5 to 2
- head_gain: float32 [256], replicated, may hold values from 0.1 to 1.9
- decay_rate: float32 [8], P('tp'), may hold values from 0 to 1, as said below
Outputs:
- tokens_out: bfloat16 [16384, 2048], P(('rep', 'fs', 'tp'))
Inputs may be any that keep to these rules, and one draw needn't show every extreme that they name: `decay_rate`: each head's decay per position, positive.
All inputs are finite; a program needn't handle non-finite values.
Results may differ from a plain program's by a relative error of at most 0.02.
Values may be sent and summed in bfloat16 or wider, within the bound.
No kernel may reach another device: no remote copies, remote signals or barrier semaphores. Data moves between devices by JAX's collectives and lax.ppermute only.
A program may use at most 64 MiB of HBM per device.

v0:
```python
import math
import jax
import jax.numpy as jnp
from jax import lax
from jax.sharding import Mesh, PartitionSpec as P

DK = 256
DV = 256
BLOCK = 64
EPSILON = 1e-05


def gather_weights(packed):
    rep = lax.axis_index("rep")
    half = packed.shape[0] // 2
    mine = lax.dynamic_slice_in_dim(packed, rep * half, half, axis=0)
    full = lax.all_gather(mine, ("rep", "z", "y"), axis=0, tiled=True)
    return (
        full.reshape(2, -1, half, packed.shape[1])
        .transpose(1, 0, 2, 3)
        .reshape(-1, packed.shape[1])
    )


def norm_rows(stream, gain):
    scale = lax.rsqrt(jnp.mean(stream * stream, axis=-1, keepdims=True) + EPSILON)
    return (stream * scale * gain).astype(jnp.bfloat16)


def swap_cores(array):
    return lax.ppermute(array, "core", [(0, 1), (1, 0)])


def gather_rows(rows):
    n = lax.axis_size("x")
    copies = jnp.broadcast_to(rows, (n, *rows.shape))
    own = lax.all_to_all(copies, "x", split_axis=0, concat_axis=0, tiled=True)
    own = own.reshape(-1, rows.shape[1])
    return jnp.concatenate([own, swap_cores(own)], axis=0)


def return_rows(part):
    n = lax.axis_size("x")
    half = part.shape[0] // 2
    sent = swap_cores(part[half:].astype(jnp.bfloat16))
    both = (part[:half] + sent.astype(jnp.float32)).astype(jnp.bfloat16)
    blocks = both.reshape(n, half // n, -1)
    arrived = lax.all_to_all(blocks, "x", split_axis=0, concat_axis=0, tiled=True)
    return arrived.astype(jnp.float32).sum(axis=0)


def dot(a, b):
    return jnp.dot(a, b, preferred_element_type=jnp.float32)


def dot_t(a, b):
    return lax.dot_general(a, b, (((1,), (1,)), ((), ())), preferred_element_type=jnp.float32)


def positions(rows):
    n = lax.axis_size("x")
    core = lax.axis_index("core")
    r = jnp.arange(n * rows, dtype=jnp.int32)
    first = r // rows * (2 * rows) + r % rows
    return jnp.concatenate([first + core * rows, first + (1 - core) * rows])


def retain(query, key_rows, value, decay_rate, head_gain, pos):
    apart = jnp.abs(pos[:, None] - pos[None, :]).astype(jnp.float32)
    seen = pos[None, :] // BLOCK <= pos[:, None] // BLOCK
    decay = jnp.where(seen, jnp.exp(-decay_rate[0] * apart), 0.0)
    scores = (dot_t(query, key_rows) * decay).astype(jnp.bfloat16)
    retained = dot(scores, value)
    centred = retained - jnp.mean(retained, axis=-1, keepdims=True)
    scale = lax.rsqrt(jnp.mean(centred * centred, axis=-1, keepdims=True) + EPSILON)
    return (centred * scale * head_gain).astype(jnp.bfloat16)


def on_device(
    tokens_in,
    norm_gains,
    gate_w,
    gate_scale,
    up_w,
    up_scale,
    down_w,
    down_scale,
    query_w,
    query_scale,
    key_w,
    key_scale,
    value_w,
    value_scale,
    out_w,
    out_scale,
    head_gain,
    decay_rate,
):

    def low(w):
        return w.astype(jnp.bfloat16)

    down_t = low(low(down_w).T.astype(jnp.float32) * down_scale[:, None])
    out_t = low(low(out_w).T.astype(jnp.float32) * out_scale[:, None])
    pieces = [low(gate_w), low(up_w), down_t, low(query_w), low(key_w), low(value_w), out_t]
    packed = jnp.concatenate(pieces, axis=1)
    full = gather_weights(packed)
    at, parts = (0, [])
    for p in pieces:
        parts.append(full[:, at : at + p.shape[1]])
        at += p.shape[1]
    gate_f, up_f, down_f, query_f, key_f, value_f, out_f = parts

    def feed_forward(stream, gain):
        rows = gather_rows(norm_rows(stream, gain))
        gate = dot(rows, gate_f) * gate_scale
        up = dot(rows, up_f) * up_scale
        hidden = low(jax.nn.silu(gate) * up)
        return return_rows(dot_t(hidden, down_f))

    stream = tokens_in.astype(jnp.float32)
    stream = stream + 0.5 * feed_forward(stream, norm_gains[0])
    rows = gather_rows(norm_rows(stream, norm_gains[1]))
    query = low(dot(rows, query_f) * query_scale)
    key_rows = low(dot(rows, key_f) * key_scale / math.sqrt(DK))
    value = low(dot(rows, value_f) * value_scale)
    mixed = retain(query, key_rows, value, decay_rate, head_gain, positions(tokens_in.shape[0]))
    stream = stream + return_rows(dot_t(mixed, out_f))
    stream = stream + 0.5 * feed_forward(stream, norm_gains[2])
    return stream.astype(jnp.bfloat16)


def solution(mesh):
    devices = mesh.devices
    reps, fs, tp = devices.shape
    fine = Mesh(devices.reshape(reps, fs // 4, 4, tp // 2, 2), ("rep", "z", "y", "x", "core"))
    F, T = (("z", "y"), ("x", "core"))
    rows = P(("rep", "z", "y", "x", "core"), None)
    wide, tall, cols, depth = (P(F, T), P(T, F), P(T), P(F))
    placed = (
        rows,
        P(),
        wide,
        cols,
        wide,
        cols,
        tall,
        depth,
        wide,
        cols,
        wide,
        cols,
        wide,
        cols,
        tall,
        depth,
        P(),
        cols,
    )
    return jax.shard_map(on_device, mesh=fine, in_specs=placed, out_specs=rows, check_vma=False)
```

profile of v0, /device:TPU:1, one launch (start us, length us, event | category | flops | bytes accessed | tf_op | source)
XLA Modules:
  0.0 294.2 jit_solution(15299229404249725897)
XLA Ops:
  7.4 0.9 convert_dynamic-update-slice_fusion
  8.3 1.0 fusion.71
  11.9 0.9 fusion.73
  13.5 1.0 fusion.38
  14.6 0.9 fusion.89
  15.5 1.0 fusion.40
  16.5 11.6 %all_to_all.30 = bf16[4,32,2048]{2,1,0:T(8,128)(2,1)S(1)} all-to-all(bf16[4,32,2048]{2,1,0:T(8,128)(2,1)S(1)} %broadcast_in_dim.9), channel_id=1, replica_groups=mesh['rep'=2,'z'=8,'y'=4,'x'=4,'core'=2] {'x'}, dimensions={0} | all-to-all | bytes 1048576 | tf_op jit(solution)/shard_map/all_to_all | solution.py:37
  28.1 7.7 %collective-permute-start = (bf16[128,2048]{1,0:T(8,128)(2,1)S(1)}, bf16[128,2048]{1,0:T(8,128)(2,1)S(1)}, u32[]{:S(2)}, u32[]{:S(2)}) collective-permute-start(bf16[128,2048]{1,0:T(8,128)(2,1)S(1)} %bitcast.41), channel_id=1, source_target_pairs={{0,1},{1,0},{2,3},{3,2},{4,5},{5,4},{6,7},{7,6},{8,9},{9,8},{10,11... | collective-permute-start | bytes 1572872 | tf_op jit(solution)/shard_map/ppermute | solution.py:31
  35.8 133.1 %all-gather.2.cloned.1.call-done = bf16[2048,2176]{1,0:T(8,128)(2,1)} async-done(((bf16[32,2176]{1,0:T(8,128)(2,1)}), bf16[2048,2176]{1,0:T(8,128)(2,1)}) %all-gather.2.cloned.1.call-update) | async-done | bytes 8912912 | tf_op jit(solution)/shard_map/all_gather | solution.py:17
  168.9 8.2 %copy.19 = bf16[32,2,32,2176]{3,2,1,0:T(8,128)(2,1)} copy(bf16[32,2,32,2176]{3,2,0,1:T(8,128)(2,1)} %bitcast.33) | data formatting | bytes 17825792 | tf_op jit(solution)/shard_map/transpose | solution.py:20
  177.1 2.9 fusion.12
  180.1 3.4 %fusion.2 = f32[256,2048]{1,0:T(8,128)S(1)} fusion(bf16[2048,2176]{1,0:T(8,128)(2,1)} %bitcast.26, f32[256,384]{1,0:T(8,128)} %fusion.12, bf16[128,2048]{1,0:T(8,128)(2,1)S(1)} %collective-permute-done, bf16[128,2048]{1,0:T(8,128)(2,1)S(1)} %bitcast.43, f32[384]{0:T(512)S(1)} %copy-done.5), kind=kOutput, calls=%fused_computation.2 | convolution fusion | flops 808091648 | bytes 6686208 | tf_op jit(solution)/shard_map/dot_general | solution.py:57
  183.5 10.4 %collective-permute-start.1 = (bf16[128,2048]{1,0:T(8,128)(2,1)S(1)}, bf16[128,2048]{1,0:T(8,128)(2,1)S(1)}, u32[]{:S(2)}, u32[]{:S(2)}) collective-permute-start(bf16[128,2048]{1,0:T(8,128)(2,1)S(1)} %slice.130), channel_id=1, source_target_pairs={{0,1},{1,0},{2,3},{3,2},{4,5},{5,4},{6,7},{7,6},{8,9},{9,8},{10,11... | collective-permute-start | bytes 1572872 | tf_op jit(solution)/shard_map/ppermute | solution.py:31
  193.9 1.5 collective-permute-done.1
  195.6 12.4 %all_to_all.31 = bf16[4,32,2048]{2,1,0:T(8,128)(2,1)S(1)} all-to-all(bf16[4,32,2048]{2,1,0:T(8,128)(2,1)S(1)} %bitcast.34), channel_id=1, replica_groups=mesh['rep'=2,'z'=8,'y'=4,'x'=4,'core'=2] {'x'}, dimensions={0} | all-to-all | bytes 1048576 | tf_op jit(solution)/shard_map/all_to_all | solution.py:48
  208.3 10.2 %all_to_all.32 = bf16[4,32,2048]{2,1,0:T(8,128)(2,1)S(1)} all-to-all(bf16[4,32,2048]{2,1,0:T(8,128)(2,1)S(1)} %broadcast_in_dim.10), channel_id=1, replica_groups=mesh['rep'=2,'z'=8,'y'=4,'x'=4,'core'=2] {'x'}, dimensions={0} | all-to-all | bytes 1048576 | tf_op jit(solution)/shard_map/all_to_all | solution.py:37
  218.5 4.7 %collective-permute-start.2 = (bf16[128,2048]{1,0:T(8,128)(2,1)S(1)}, bf16[128,2048]{1,0:T(8,128)(2,1)S(1)}, u32[]{:S(2)}, u32[]{:S(2)}) collective-permute-start(bf16[128,2048]{1,0:T(8,128)(2,1)S(1)} %bitcast.37), channel_id=1, source_target_pairs={{0,1},{1,0},{2,3},{3,2},{4,5},{5,4},{6,7},{7,6},{8,9},{9,8},{10,11... | collective-permute-start | bytes 1572872 | tf_op jit(solution)/shard_map/ppermute | solution.py:31
  224.7 1.7 fusion.26
  226.4 1.7 fusion.25
  228.1 1.7 fusion.27
  230.3 1.8 fusion.32
  232.2 2.3 collective-permute-start.3
  234.5 1.5 collective-permute-done.3
  236.1 11.6 %all_to_all.33 = bf16[4,32,2048]{2,1,0:T(8,128)(2,1)S(1)} all-to-all(bf16[4,32,2048]{2,1,0:T(8,128)(2,1)S(1)} %bitcast.35), channel_id=1, replica_groups=mesh['rep'=2,'z'=8,'y'=4,'x'=4,'core'=2] {'x'}, dimensions={0} | all-to-all | bytes 1048576 | tf_op jit(solution)/shard_map/all_to_all | solution.py:48
  248.2 10.7 %all_to_all.34 = bf16[4,32,2048]{2,1,0:T(8,128)(2,1)S(1)} all-to-all(bf16[4,32,2048]{2,1,0:T(8,128)(2,1)S(1)} %broadcast_in_dim.12), channel_id=1, replica_groups=mesh['rep'=2,'z'=8,'y'=4,'x'=4,'core'=2] {'x'}, dimensions={0} | all-to-all | bytes 1048576 | tf_op jit(solution)/shard_map/all_to_all | solution.py:37
  258.9 4.1 %collective-permute-start.4 = (bf16[128,2048]{1,0:T(8,128)(2,1)S(1)}, bf16[128,2048]{1,0:T(8,128)(2,1)S(1)}, u32[]{:S(2)}, u32[]{:S(2)}) collective-permute-start(bf16[128,2048]{1,0:T(8,128)(2,1)S(1)} %bitcast.44), channel_id=1, source_target_pairs={{0,1},{1,0},{2,3},{3,2},{4,5},{5,4},{6,7},{7,6},{8,9},{9,8},{10,11... | collective-permute-start | bytes 1572872 | tf_op jit(solution)/shard_map/ppermute | solution.py:31
  263.0 1.5 collective-permute-done.4
  265.4 2.1 fusion.15
  267.6 3.4 %fusion = f32[256,2048]{1,0:T(8,128)S(1)} fusion(bf16[2048,2176]{1,0:T(8,128)(2,1)} %bitcast.32, f32[256,384]{1,0:T(8,128)S(1)} %fusion.15, bf16[128,2048]{1,0:T(8,128)(2,1)} %copy-done.2, bf16[128,2048]{1,0:T(8,128)(2,1)S(1)} %bitcast.46, f32[384]{0:T(512)S(1)} %copy-done.6), kind=kOutput, calls=%fused_computation | convolution fusion | flops 808091648 | bytes 6686208 | tf_op jit(solution)/shard_map/dot_general | solution.py:57
  271.0 2.3 collective-permute-start.5
  273.3 1.5 collective-permute-done.5
  275.0 11.6 %all_to_all.35 = bf16[4,32,2048]{2,1,0:T(8,128)(2,1)S(1)} all-to-all(bf16[4,32,2048]{2,1,0:T(8,128)(2,1)S(1)} %bitcast.36), channel_id=1, replica_groups=mesh['rep'=2,'z'=8,'y'=4,'x'=4,'core'=2] {'x'}, dimensions={0} | all-to-all | bytes 1048576 | tf_op jit(solution)/shard_map/all_to_all | solution.py:48
  (55 shorter events, 8.6 us)
Async XLA Ops:
  6.5 162.3 %all-gather.2.cloned.1.call-start = ((), (), s32[]{:S(2)}) async-start(), calls=%async_computation.6 | async-start | bytes 9052160 | tf_op jit(solution)/shard_map/all_gather | solution.py:17
  28.1 149.0 %collective-permute-start = (bf16[128,2048]{1,0:T(8,128)(2,1)S(1)}, bf16[128,2048]{1,0:T(8,128)(2,1)S(1)}, u32[]{:S(2)}, u32[]{:S(2)}) collective-permute-start(bf16[128,2048]{1,0:T(8,128)(2,1)S(1)} %bitcast.41), channel_id=1, source_target_pairs={{0,1},{1,0},{2,3},{3,2},{4,5},{5,4},{6,7},{7,6},{8,9},{9,8},{10,11... | collective-permute-start | bytes 1572872 | tf_op jit(solution)/shard_map/ppermute | solution.py:31
  168.9 8.2 %copy-start.3 = (f32[384]{0:T(512)S(1)}, f32[384]{0:T(512)}, u32[]{:S(2)}) copy-start(f32[384]{0:T(512)} %param.21) | copy-start | bytes 4612
  177.1 2.9 %copy-start.5 = (f32[384]{0:T(512)S(1)}, f32[384]{0:T(512)}, u32[]{:S(2)}) copy-start(f32[384]{0:T(512)} %param.23) | copy-start | bytes 4612
  183.5 24.5 %copy-start = (bf16[32,2048]{1,0:T(8,128)(2,1)S(1)}, bf16[32,2048]{1,0:T(8,128)(2,1)}, u32[]{:S(2)}) copy-start(bf16[32,2048]{1,0:T(8,128)(2,1)} %param.18) | copy-start | bytes 393220
  183.5 11.9 %collective-permute-start.1 = (bf16[128,2048]{1,0:T(8,128)(2,1)S(1)}, bf16[128,2048]{1,0:T(8,128)(2,1)S(1)}, u32[]{:S(2)}, u32[]{:S(2)}) collective-permute-start(bf16[128,2048]{1,0:T(8,128)(2,1)S(1)} %slice.130), channel_id=1, source_target_pairs={{0,1},{1,0},{2,3},{3,2},{4,5},{5,4},{6,7},{7,6},{8,9},{9,8},{10,11... | collective-permute-start | bytes 1572872 | tf_op jit(solution)/shard_map/ppermute | solution.py:31
  195.5 29.2 %copy-start.7 = (f32[256]{0:T(256)S(1)}, f32[256]{0:T(256)}, u32[]{:S(2)}) copy-start(f32[256]{0:T(256)} %param.29) | copy-start | bytes 3076
  218.5 7.9 %copy-start.8 = (f32[256]{0:T(256)S(1)}, f32[256]{0:T(256)}, u32[]{:S(2)}) copy-start(f32[256]{0:T(256)} %param.27) | copy-start | bytes 3076
  218.5 6.2 %collective-permute-start.2 = (bf16[128,2048]{1,0:T(8,128)(2,1)S(1)}, bf16[128,2048]{1,0:T(8,128)(2,1)S(1)}, u32[]{:S(2)}, u32[]{:S(2)}) collective-permute-start(bf16[128,2048]{1,0:T(8,128)(2,1)S(1)} %bitcast.37), channel_id=1, source_target_pairs={{0,1},{1,0},{2,3},{3,2},{4,5},{5,4},{6,7},{7,6},{8,9},{9,8},{10,11... | collective-permute-start | bytes 1572872 | tf_op jit(solution)/shard_map/ppermute | solution.py:31
  226.4 1.7 copy-start.9
  228.1 2.2 copy-start.1
  232.2 3.8 %collective-permute-start.3 = (bf16[128,2048]{1,0:T(8,128)(2,1)S(1)}, bf16[128,2048]{1,0:T(8,128)(2,1)S(1)}, u32[]{:S(2)}, u32[]{:S(2)}) collective-permute-start(bf16[128,2048]{1,0:T(8,128)(2,1)S(1)} %slice.129), channel_id=1, source_target_pairs={{0,1},{1,0},{2,3},{3,2},{4,5},{5,4},{6,7},{7,6},{8,9},{9,8},{10,11... | collective-permute-start | bytes 1572872 | tf_op jit(solution)/shard_map/ppermute | solution.py:31
  247.7 17.7 %copy-start.4 = (f32[384]{0:T(512)S(1)}, f32[384]{0:T(512)}, u32[]{:S(2)}) copy-start(f32[384]{0:T(512)} %param.21) | copy-start | bytes 4612
  258.9 8.7 %copy-start.6 = (f32[384]{0:T(512)S(1)}, f32[384]{0:T(512)}, u32[]{:S(2)}) copy-start(f32[384]{0:T(512)} %param.23) | copy-start | bytes 4612
  258.9 5.6 %collective-permute-start.4 = (bf16[128,2048]{1,0:T(8,128)(2,1)S(1)}, bf16[128,2048]{1,0:T(8,128)(2,1)S(1)}, u32[]{:S(2)}, u32[]{:S(2)}) collective-permute-start(bf16[128,2048]{1,0:T(8,128)(2,1)S(1)} %bitcast.44), channel_id=1, source_target_pairs={{0,1},{1,0},{2,3},{3,2},{4,5},{5,4},{6,7},{7,6},{8,9},{9,8},{10,11... | collective-permute-start | bytes 1572872 | tf_op jit(solution)/shard_map/ppermute | solution.py:31
  264.5 0.9 copy-start.2
  271.0 3.8 %collective-permute-start.5 = (bf16[128,2048]{1,0:T(8,128)(2,1)S(1)}, bf16[128,2048]{1,0:T(8,128)(2,1)S(1)}, u32[]{:S(2)}, u32[]{:S(2)}) collective-permute-start(bf16[128,2048]{1,0:T(8,128)(2,1)S(1)} %slice.128), channel_id=1, source_target_pairs={{0,1},{1,0},{2,3},{3,2},{4,5},{5,4},{6,7},{7,6},{8,9},{9,8},{10,11... | collective-permute-start | bytes 1572872 | tf_op jit(solution)/shard_map/ppermute | solution.py:31
Sparse Core Ops, SparseCore 0:
  13.6 155.1 all-gather.1
where the time goes:
time: 295 us; the launch traced here: 294 us
  waiting for transfers between devices  140 us (47%)
  blocking collectives  68 us (23%)
  starting transfers between devices  31.4 us (11%)
  matrix products  19.1 us (6%)
  between operations  14.4 us (5%)
  local copies, waits for them, and re-layouts  11 us (4%)
  other arithmetic  10.2 us (3%)
    all_gather x1, waiting for transfers between devices, gather_weights(): full = lax.all_gather(mine, ('rep', 'z', 'y'), axis=0, tiled=True)  133 us
    all_to_all x3, blocking collectives, return_rows(): lax.all_to_all(blocks, 'x', split_axis=0, concat_axis=0, tiled=True)  35.6 us
    all_to_all x3, blocking collectives, gather_rows(): own = lax.all_to_all(copies, 'x', split_axis=0, concat_axis=0, tiled=True)  32.5 us
    ppermute x6, starting transfers between devices, swap_cores(): return lax.ppermute(array, 'core', [(0, 1), (1, 0)])  31.4 us
    dot_general x6, matrix products, dot(): return jnp.dot(a, b, preferred_element_type=jnp.float32)  10.5 us
    dot_general x3, matrix products, dot_t(): lax.dot_general(a, b, (((1,), (1,)), ((), ())), preferred_element_type=jn...  8.57 us
    transpose x1, local copies, waits for them, and re-layouts, gather_weights(): return full.reshape(2, -1, half, packed.shape[1]).transpose(1, 0, 2, 3).r...  8.24 us
    ppermute x6, waiting for transfers between devices, swap_cores(): return lax.ppermute(array, 'core', [(0, 1), (1, 0)])  6.89 us
  transfers between devices with their start and end apart: 7, of which 6 were waited for; matrix products, arithmetic and copies ran while one was open for 4% of the time, Pallas kernels for 0%

commit v1 on v0

--- a/solution.py
+++ b/solution.py
@@ -14,7 +14,12 @@
     rep = lax.axis_index("rep")
     half = packed.shape[0] // 2
     mine = lax.dynamic_slice_in_dim(packed, rep * half, half, axis=0)
-    full = lax.all_gather(mine, ("rep", "z", "y"), axis=0, tiled=True)
+    full = jnp.concatenate(
+        lax.all_to_all(
+            jnp.stack([mine] * lax.axis_size(("rep", "z", "y"))), ("rep", "z", "y"), 0, 0
+        ),
+        axis=0,
+    )
     return (
         full.reshape(2, -1, half, packed.shape[1])
         .transpose(1, 0, 2, 3)

time: 295 us -> 543 us (1.84)
  waiting for transfers between devices: 140 us -> 393 us
  starting transfers between devices: 31.4 us -> 53.4 us
  between operations: 14.4 us -> 1.1 us
  blocking collectives: 68 us -> 56.3 us
  other arithmetic: 10.2 us -> 4.14 us
    all_to_all x0 -> x2, waiting for transfers between devices: none -> 386 us  [the longest x1 379 us: gather_weights(): lax.all_to_all(jnp.stack([mine] * lax.axis_size(('rep', 'z', 'y'))), ('re...]
    all_gather x1 -> x0, waiting for transfers between devices: 133 us -> none  [gather_weights(): full = lax.all_gather(mine, ('rep', 'z', 'y'), axis=0, tiled=True)]
    all_to_all x0 -> x2, starting transfers between devices: none -> 24.9 us  [the longest x1 20.1 us: gather_weights(): lax.all_to_all(jnp.stack([mine] * lax.axis_size(('rep', 'z', 'y'))), ('re...]
    all_to_all x3 -> x2, blocking collectives: 32.5 us -> 21.5 us  [gather_rows(): own = lax.all_to_all(copies, 'x', split_axis=0, concat_axis=0, tiled=True)]
  transfers between devices with their start and end apart: 7 -> 8, of which waited for: 6 -> 7; matrix products, arithmetic and copies ran while one was open for 4% -> 2% of each run, Pallas kernels for 0% -> 0%
where the time goes in v1:
time: 543 us; the launch traced here: 542 us
  waiting for transfers between devices  393 us (72%)
  blocking collectives  56.3 us (10%)
  starting transfers between devices  53.4 us (10%)
  matrix products  19.2 us (4%)
  local copies, waits for them, and re-layouts  15.3 us (3%)
    all_to_all x1, waiting for transfers between devices, gather_weights(): lax.all_to_all(jnp.stack([mine] * lax.axis_size(('rep', 'z', 'y'))), ('re...  379 us
    all_to_all x3, blocking collectives, return_rows(): lax.all_to_all(blocks, 'x', split_axis=0, concat_axis=0, tiled=True)  34.8 us
    ppermute x6, starting transfers between devices, swap_cores(): return lax.ppermute(array, 'core', [(0, 1), (1, 0)])  28.5 us
    all_to_all x2, blocking collectives, gather_rows(): own = lax.all_to_all(copies, 'x', split_axis=0, concat_axis=0, tiled=True)  21.5 us
    all_to_all x1, starting transfers between devices, gather_weights(): lax.all_to_all(jnp.stack([mine] * lax.axis_size(('rep', 'z', 'y'))), ('re...  20.1 us
  transfers between devices with their start and end apart: 8, of which 7 were waited for; matrix products, arithmetic and copies ran while one was open for 2% of the time, Pallas kernels for 0%

profile of v1, /device:TPU:1, one launch (start us, length us, event | category | flops | bytes accessed | tf_op | source)
XLA Modules:
  0.0 542.3 jit_solution(4056291673577262218)
XLA Ops:
  0.1 0.9 fusion.89
  1.0 1.0 fusion.38
  2.0 1.0 fusion.40
  3.9 4.8 all-to-all-start
  9.1 6.6 %all-to-all-done = bf16[4,32,2048]{2,1,0:T(8,128)(2,1)S(1)} async-done(((bf16[4,32,2048]{2,1,0:T(8,128)(2,1)}), bf16[4,32,2048]{2,1,0:T(8,128)(2,1)S(1)}, u32[]{:S(2)}, u32[]{:S(2)}) %all-to-all-start) | async-done | bytes 524320 | tf_op jit(solution)/shard_map/all_to_all | solution.py:42
  15.7 4.0 stack.2
  19.7 20.1 %all-to-all-start.1 = ((bf16[64,32,2176]{2,1,0:T(8,128)(2,1)}), bf16[64,32,2176]{2,1,0:T(8,128)(2,1)}, u32[]{:S(2)}, u32[]{:S(2)}) async-start(bf16[64,32,2176]{2,1,0:T(8,128)(2,1)} %stack.2), calls=%async_computation.1 | async-start | bytes 17825792 | tf_op jit(solution)/shard_map/all_to_all | solution.py:18
  39.8 4.3 collective-permute-start
  44.1 379.4 %all-to-all-done.1 = bf16[64,32,2176]{2,1,0:T(8,128)(2,1)} async-done(((bf16[64,32,2176]{2,1,0:T(8,128)(2,1)}), bf16[64,32,2176]{2,1,0:T(8,128)(2,1)}, u32[]{:S(2)}, u32[]{:S(2)}) %all-to-all-start.1) | async-done | bytes 8912928 | tf_op jit(solution)/shard_map/all_to_all | solution.py:18
  423.6 8.3 %copy.19 = bf16[32,2,32,2176]{3,2,1,0:T(8,128)(2,1)} copy(bf16[32,2,32,2176]{3,2,0,1:T(8,128)(2,1)} %bitcast.5) | data formatting | bytes 17825792 | tf_op jit(solution)/shard_map/transpose | solution.py:25
  431.8 2.9 fusion.12
  434.8 3.4 fusion.2
  438.2 11.5 %collective-permute-start.1 = (bf16[128,2048]{1,0:T(8,128)(2,1)S(1)}, bf16[128,2048]{1,0:T(8,128)(2,1)S(1)}, u32[]{:S(2)}, u32[]{:S(2)}) collective-permute-start(bf16[128,2048]{1,0:T(8,128)(2,1)S(1)} %slice.130), channel_id=1, source_target_pairs={{0,1},{1,0},{2,3},{3,2},{4,5},{5,4},{6,7},{7,6},{8,9},{9,8},{10,11... | collective-permute-start | bytes 1572872 | tf_op jit(solution)/shard_map/ppermute | solution.py:36
  449.8 1.5 collective-permute-done.1
  451.4 11.6 %all_to_all.35 = bf16[4,32,2048]{2,1,0:T(8,128)(2,1)S(1)} all-to-all(bf16[4,32,2048]{2,1,0:T(8,128)(2,1)S(1)} %bitcast.33), channel_id=1, replica_groups=mesh['rep'=2,'z'=8,'y'=4,'x'=4,'core'=2] {'x'}, dimensions={0} | all-to-all | bytes 1048576 | tf_op jit(solution)/shard_map/all_to_all | solution.py:53
  463.4 10.7 %all_to_all.36 = bf16[4,32,2048]{2,1,0:T(8,128)(2,1)S(1)} all-to-all(bf16[4,32,2048]{2,1,0:T(8,128)(2,1)S(1)} %broadcast_in_dim.10), channel_id=1, replica_groups=mesh['rep'=2,'z'=8,'y'=4,'x'=4,'core'=2] {'x'}, dimensions={0} | all-to-all | bytes 1048576 | tf_op jit(solution)/shard_map/all_to_all | solution.py:42
  474.2 4.1 collective-permute-start.2
  479.8 1.7 fusion.26
  481.5 1.7 fusion.25
  483.3 1.7 fusion.27
  485.5 1.8 fusion.32
  487.4 2.3 collective-permute-start.3
  489.7 1.5 collective-permute-done.3
  491.3 11.6 %all_to_all.37 = bf16[4,32,2048]{2,1,0:T(8,128)(2,1)S(1)} all-to-all(bf16[4,32,2048]{2,1,0:T(8,128)(2,1)S(1)} %bitcast.34), channel_id=1, replica_groups=mesh['rep'=2,'z'=8,'y'=4,'x'=4,'core'=2] {'x'}, dimensions={0} | all-to-all | bytes 1048576 | tf_op jit(solution)/shard_map/all_to_all | solution.py:53
  503.3 10.7 %all_to_all.38 = bf16[4,32,2048]{2,1,0:T(8,128)(2,1)S(1)} all-to-all(bf16[4,32,2048]{2,1,0:T(8,128)(2,1)S(1)} %broadcast_in_dim.12), channel_id=1, replica_groups=mesh['rep'=2,'z'=8,'y'=4,'x'=4,'core'=2] {'x'}, dimensions={0} | all-to-all | bytes 1048576 | tf_op jit(solution)/shard_map/all_to_all | solution.py:42
  514.1 4.0 collective-permute-start.4
  518.1 1.5 collective-permute-done.4
  520.4 2.1 fusion.15
  522.6 3.4 fusion
  526.0 2.3 collective-permute-start.5
  528.3 1.5 collective-permute-done.5
  530.0 11.6 %all_to_all.39 = bf16[4,32,2048]{2,1,0:T(8,128)(2,1)S(1)} all-to-all(bf16[4,32,2048]{2,1,0:T(8,128)(2,1)S(1)} %bitcast.35), channel_id=1, replica_groups=mesh['rep'=2,'z'=8,'y'=4,'x'=4,'core'=2] {'x'}, dimensions={0} | all-to-all | bytes 1048576 | tf_op jit(solution)/shard_map/all_to_all | solution.py:53
  (70 shorter events, 5.4 us)
Async XLA Ops:
  0.0 8.8 %copy-start.1 = (f32[64,384]{1,0:T(8,128)S(1)}, f32[64,384]{1,0:T(8,128)}, u32[]{:S(2)}) copy-start(f32[64,384]{1,0:T(8,128)} %param.20) | copy-start | bytes 294916
  0.0 8.8 %copy-start.2 = (f32[64,384]{1,0:T(8,128)S(1)}, f32[64,384]{1,0:T(8,128)}, u32[]{:S(2)}) copy-start(f32[64,384]{1,0:T(8,128)} %param.22) | copy-start | bytes 294916
  0.0 8.8 %copy-start.3 = (f32[384,64]{0,1:T(8,128)S(1)}, f32[384,64]{0,1:T(8,128)}, u32[]{:S(2)}) copy-start(f32[384,64]{0,1:T(8,128)} %param.24) | copy-start | bytes 294916
  0.0 8.8 %copy-start.9 = (f32[64]{0:T(128)S(1)}, f32[64]{0:T(128)}, u32[]{:S(2)}) copy-start(f32[64]{0:T(128)} %param.25) | copy-start | bytes 772
  0.0 8.9 %copy-start.4 = (f32[64,256]{1,0:T(8,128)S(1)}, f32[64,256]{1,0:T(8,128)}, u32[]{:S(2)}) copy-start(f32[64,256]{1,0:T(8,128)} %param.26) | copy-start | bytes 196612
  0.0 8.9 %copy-start.5 = (f32[64,256]{1,0:T(8,128)S(1)}, f32[64,256]{1,0:T(8,128)}, u32[]{:S(2)}) copy-start(f32[64,256]{1,0:T(8,128)} %param.28) | copy-start | bytes 196612
  0.0 8.9 %copy-start.6 = (f32[64,256]{1,0:T(8,128)S(1)}, f32[64,256]{1,0:T(8,128)}, u32[]{:S(2)}) copy-start(f32[64,256]{1,0:T(8,128)} %param.30) | copy-start | bytes 196612
  0.0 8.9 %copy-start.7 = (f32[256,64]{0,1:T(8,128)S(1)}, f32[256,64]{0,1:T(8,128)}, u32[]{:S(2)}) copy-start(f32[256,64]{0,1:T(8,128)} %param.32) | copy-start | bytes 196612
  0.1 8.9 %copy-start.10 = (f32[64]{0:T(128)S(1)}, f32[64]{0:T(128)}, u32[]{:S(2)}) copy-start(f32[64]{0:T(128)} %param.33) | copy-start | bytes 772
  3.9 11.8 %all-to-all-start = ((bf16[4,32,2048]{2,1,0:T(8,128)(2,1)}), bf16[4,32,2048]{2,1,0:T(8,128)(2,1)S(1)}, u32[]{:S(2)}, u32[]{:S(2)}) async-start(bf16[4,32,2048]{2,1,0:T(8,128)(2,1)} %broadcast_in_dim.9), calls=%async_computation | async-start | bytes 1048576 | tf_op jit(solution)/shard_map/all_to_all | solution.py:42
  19.7 403.8 %all-to-all-start.1 = ((bf16[64,32,2176]{2,1,0:T(8,128)(2,1)}), bf16[64,32,2176]{2,1,0:T(8,128)(2,1)}, u32[]{:S(2)}, u32[]{:S(2)}) async-start(bf16[64,32,2176]{2,1,0:T(8,128)(2,1)} %stack.2), calls=%async_computation.1 | async-start | bytes 17825792 | tf_op jit(solution)/shard_map/all_to_all | solution.py:18
  39.8 392.0 %collective-permute-start = (bf16[128,2048]{1,0:T(8,128)(2,1)S(1)}, bf16[128,2048]{1,0:T(8,128)(2,1)S(1)}, u32[]{:S(2)}, u32[]{:S(2)}) collective-permute-start(bf16[128,2048]{1,0:T(8,128)(2,1)S(1)} %bitcast.36), channel_id=1, source_target_pairs={{0,1},{1,0},{2,3},{3,2},{4,5},{5,4},{6,7},{7,6},{8,9},{9,8},{10,11... | collective-permute-start | bytes 1572872 | tf_op jit(solution)/shard_map/ppermute | solution.py:36
  423.6 8.3 %copy-start.12 = (f32[384]{0:T(512)S(1)}, f32[384]{0:T(512)}, u32[]{:S(2)}) copy-start(f32[384]{0:T(512)} %param.21) | copy-start | bytes 4612
  431.8 2.9 copy-start.13
  438.2 24.9 %copy-start = (bf16[32,2048]{1,0:T(8,128)(2,1)S(1)}, bf16[32,2048]{1,0:T(8,128)(2,1)}, u32[]{:S(2)}) copy-start(bf16[32,2048]{1,0:T(8,128)(2,1)} %param.18) | copy-start | bytes 393220
  438.2 13.0 %collective-permute-start.1 = (bf16[128,2048]{1,0:T(8,128)(2,1)S(1)}, bf16[128,2048]{1,0:T(8,128)(2,1)S(1)}, u32[]{:S(2)}, u32[]{:S(2)}) collective-permute-start(bf16[128,2048]{1,0:T(8,128)(2,1)S(1)} %slice.130), channel_id=1, source_target_pairs={{0,1},{1,0},{2,3},{3,2},{4,5},{5,4},{6,7},{7,6},{8,9},{9,8},{10,11... | collective-permute-start | bytes 1572872 | tf_op jit(solution)/shard_map/ppermute | solution.py:36
  451.4 28.4 %copy-start.14 = (f32[256]{0:T(256)S(1)}, f32[256]{0:T(256)}, u32[]{:S(2)}) copy-start(f32[256]{0:T(256)} %param.29) | copy-start | bytes 3076
  474.2 7.4 %copy-start.15 = (f32[256]{0:T(256)S(1)}, f32[256]{0:T(256)}, u32[]{:S(2)}) copy-start(f32[256]{0:T(256)} %param.27) | copy-start | bytes 3076
  474.2 5.6 %collective-permute-start.2 = (bf16[128,2048]{1,0:T(8,128)(2,1)S(1)}, bf16[128,2048]{1,0:T(8,128)(2,1)S(1)}, u32[]{:S(2)}, u32[]{:S(2)}) collective-permute-start(bf16[128,2048]{1,0:T(8,128)(2,1)S(1)} %bitcast.39), channel_id=1, source_target_pairs={{0,1},{1,0},{2,3},{3,2},{4,5},{5,4},{6,7},{7,6},{8,9},{9,8},{10,11... | collective-permute-start | bytes 1572872 | tf_op jit(solution)/shard_map/ppermute | solution.py:36
  481.5 1.7 copy-start.16
  483.2 2.2 copy-start.8
  487.4 3.8 collective-permute-start.3
  514.1 5.5 %collective-permute-start.4 = (bf16[128,2048]{1,0:T(8,128)(2,1)S(1)}, bf16[128,2048]{1,0:T(8,128)(2,1)S(1)}, u32[]{:S(2)}, u32[]{:S(2)}) collective-permute-start(bf16[128,2048]{1,0:T(8,128)(2,1)S(1)} %bitcast.43), channel_id=1, source_target_pairs={{0,1},{1,0},{2,3},{3,2},{4,5},{5,4},{6,7},{7,6},{8,9},{9,8},{10,11... | collective-permute-start | bytes 1572872 | tf_op jit(solution)/shard_map/ppermute | solution.py:36
  519.6 0.8 copy-start.11
  526.0 3.8 collective-permute-start.5
